TPU v7x, 32 devices: a whole 2x2x4 slice. The times are simulated.
32 devices in a mesh: grp: 2 (over y), fs: 4 (over z), tp: 4 (over x, core).
Axes of the slice: x: 2, y: 2, z: 4, core: 2. Of those that a mesh axis runs over, the one named last changes fastest.
Arguments:
- tokens: bfloat16 [4096, 2048], P(('grp', 'fs', 'tp')), parts along dimension 0, may hold values from -6 to 6
- up_master: float32 [2048, 4096], P('fs', 'tp'), may hold values from -0.125 to 0.125
- down_master: float32 [4096, 2048], P('fs', 'tp'), may hold values from -0.09375 to 0.09375
- norm_gain: float32 [2048], P('fs'), may hold values from 0.1 to 1.9
Outputs:
- up_weights: bfloat16 [4096, 4096], P('grp', 'tp'), parts along dimension 0
- down_weights: bfloat16 [8192, 2048], P(('grp', 'tp')), parts along dimension 0
- mlp_output: bfloat16 [4096, 2048], P(('grp', 'fs', 'tp')), parts along dimension 0
There are 2 independent parts, one for each index of `grp`. A program takes and returns all parts, laid end to end along the dimension named above; an argument that names none is the same for every part. Nothing has to cross between parts.
All inputs are finite; a program needn't handle non-finite values.
Results may differ from a plain program's by a relative error of at most 0.014.
Values may be sent and summed in bfloat16 or wider, within the bound.
A program may use at most 64 MiB of HBM per device.

v0:
```python
import jax
import jax.numpy as jnp
from jax import lax
from jax.sharding import PartitionSpec as P


def on_device(tokens, up_master, down_master, norm_gain):
    up_local = (norm_gain[:, None] * up_master).astype(jnp.bfloat16)
    down_local = down_master.astype(jnp.bfloat16)
    float_tokens = tokens.astype(jnp.float32)
    scale = lax.rsqrt(jnp.mean(float_tokens * float_tokens, axis=-1, keepdims=True) + 1e-06)
    normed_local = (float_tokens * scale).astype(jnp.bfloat16)
    normed = lax.all_gather(normed_local, "tp", axis=0, tiled=True)
    up_weights = lax.all_gather(up_local, "fs", axis=0, tiled=True)
    preact = jnp.dot(normed, up_weights, preferred_element_type=jnp.float32)
    gathered_rows = lax.all_gather(down_local, "fs", axis=0, tiled=True)
    down_weights = lax.all_to_all(gathered_rows, "tp", split_axis=0, concat_axis=1, tiled=True)
    rectified = jax.nn.relu(preact)
    hidden = (rectified * rectified).astype(jnp.bfloat16)
    mlp_output = lax.psum_scatter(
        jnp.dot(hidden, down_weights, preferred_element_type=jnp.float32).astype(jnp.bfloat16),
        "tp",
        scatter_dimension=0,
        tiled=True,
    )
    return (up_weights, down_weights, mlp_output)


def solution(mesh):
    in_specs = (P(("grp", "fs", "tp"), None), P("fs", "tp"), P("fs", "tp"), P("fs"))
    out_specs = (P("grp", "tp"), P(("grp", "tp"), None), P(("grp", "fs", "tp"), None))
    return jax.shard_map(
        on_device, mesh=mesh, in_specs=in_specs, out_specs=out_specs, check_vma=False
    )
```

profile of v0, /device:TPU:1, one launch (start us, length us, event | category | flops | bytes accessed | tf_op | source)
XLA Modules:
  0.0 261.2 jit_solution(9083774294734147993)
XLA Ops:
  7.2 0.0 copy-start.1
  7.2 0.0 all-gather.6.cloned.1.call-start
  7.2 2.7 %convert_element_type.19 = bf16[1024,512]{1,0:T(8,128)(2,1)} convert(f32[1024,512]{1,0:T(8,128)} %param.6) | non-fusion elementwise | flops 524288 | bytes 3145728 | tf_op jit(solution)/shard_map/convert_element_type | solution.py:9
  10.0 0.0 copy-start
  10.0 0.0 copy-start.2
  10.0 0.0 all-gather.6.cloned.1.call-update
  10.0 0.0 all-gather.8.cloned.1.call-start
  10.0 0.0 copy-done.1
  10.1 0.2 fusion
  10.2 1.0 fusion.1
  11.2 0.0 all-gather.8.cloned.1.call-update
  11.2 0.0 all-gather.4.cloned.1.call-start
  11.3 0.5 copy-done
  11.7 0.0 copy-done.2
  11.7 1.1 multiply_convert_fusion.1
  12.9 0.0 all-gather.4.cloned.1.call-update
  12.9 0.0 reduce-scatter.2.cloned.1.call-start
  13.0 79.9 %all-gather.6.cloned.1.call-done = bf16[4096,512]{1,0:T(8,128)(2,1)} async-done(((bf16[1024,512]{1,0:T(8,128)(2,1)}), bf16[4096,512]{1,0:T(8,128)(2,1)}) %all-gather.6.cloned.1.call-update) | async-done | bytes 4194320 | tf_op jit(solution)/shard_map/all_gather | solution.py:16
  92.8 65.2 %all_to_all.19 = bf16[4,1024,512]{2,1,0:T(8,128)(2,1)} all-to-all(bf16[4,1024,512]{2,1,0:T(8,128)(2,1)} %bitcast.9), channel_id=1, replica_groups=mesh['grp'=2,'fs'=4,'tp'=4] {'tp'}, dimensions={0} | all-to-all | bytes 8388608 | tf_op jit(solution)/shard_map/all_to_all | solution.py:17
  158.0 6.2 %copy.8 = bf16[4,1024,512]{1,2,0:T(8,128)(2,1)} copy(bf16[4,1024,512]{2,1,0:T(8,128)(2,1)} %all_to_all.19) | data formatting | bytes 8388608 | tf_op jit(solution)/shard_map/all_to_all | solution.py:17
  164.2 0.0 all-gather.8.cloned.1.call-done
  164.2 46.1 %all-gather.4.cloned.1.call-done = bf16[2048,1024]{1,0:T(8,128)(2,1)} async-done(((bf16[512,1024]{1,0:T(8,128)(2,1)}), bf16[2048,1024]{1,0:T(8,128)(2,1)}) %all-gather.4.cloned.1.call-update) | async-done | bytes 4194320 | tf_op jit(solution)/shard_map/all_gather | solution.py:14
  210.3 9.9 %convolution_convert_fusion = bf16[512,2048]{1,0:T(8,128)(2,1)} fusion(bf16[1024,2048]{0,1:T(8,128)(2,1)} %bitcast.7, bf16[512,2048]{1,0:T(8,128)(2,1)} %all-gather.8.cloned.1.call-done, bf16[2048,1024]{1,0:T(8,128)(2,1)} %all-gather.4.cloned.1.call-done), kind=kOutput, calls=%fused_computation | convolution fusion | flops 4297588736 | bytes 12582912 | tf_op jit(solution)/shard_map/dot_general | solution.py:21
  220.2 0.0 reduce-scatter.2.cloned.1.call-update
  220.2 6.5 %copy.9 = bf16[1024,2048]{1,0:T(8,128)(2,1)} copy(bf16[1024,2048]{0,1:T(8,128)(2,1)} %bitcast.8) | data formatting | bytes 8388608
  226.7 23.3 %reduce-scatter.2.cloned.1.call-done = bf16[128,2048]{1,0:T(8,128)(2,1)} async-done(((bf16[512,2048]{1,0:T(8,128)(2,1)}), bf16[128,2048]{1,0:T(8,128)(2,1)}) %reduce-scatter.2.cloned.1.call-update) | async-done | bytes 524304 | tf_op jit(solution)/shard_map/reduce_scatter | solution.py:20
  250.0 4.6 %copy.11 = bf16[2048,1024]{1,0:T(8,128)(2,1)} copy(bf16[2048,1024]{1,0:T(8,128)(2,1)} %all-gather.4.cloned.1.call-done) | data formatting | bytes 8388608
  (1 shorter events, 0.0 us)
Async XLA Ops:
  7.2 2.9 %copy-start.1 = (bf16[128,2048]{1,0:T(8,128)(2,1)S(1)}, bf16[128,2048]{1,0:T(8,128)(2,1)}, u32[]{:S(2)}) copy-start(bf16[128,2048]{1,0:T(8,128)(2,1)} %param.4) | copy-start | bytes 1572868
  7.2 85.7 %all-gather.6.cloned.1.call-start = ((), (), s32[]{:S(2)}) async-start(), calls=%async_computation.3 | async-start | bytes 5242880 | tf_op jit(solution)/shard_map/all_gather | solution.py:16
  10.0 1.8 copy-start
  10.0 1.8 copy-start.2
  10.0 154.2 %all-gather.8.cloned.1.call-start = ((), (), s32[]{:S(2)}) async-start(), calls=%async_computation.4 | async-start | bytes 2621440 | tf_op jit(solution)/shard_map/all_gather | solution.py:13
  11.2 199.1 %all-gather.4.cloned.1.call-start = ((), (), s32[]{:S(2)}) async-start(), calls=%async_computation.2 | async-start | bytes 5242880 | tf_op jit(solution)/shard_map/all_gather | solution.py:14
  12.9 237.1 %reduce-scatter.2.cloned.1.call-start = ((), (), s32[]{:S(2)}) async-start(), calls=%async_computation.5 | async-start | bytes 2621440 | tf_op jit(solution)/shard_map/reduce_scatter | solution.py:20
Sparse Core Ops, SparseCore 0:
  10.1 82.6 all-gather.5
  95.0 32.9 all-gather.7
  130.1 80.1 all-gather.3
  220.3 29.6 reduce-scatter.1
where the time goes:
time: 263 us; the launch traced here: 261 us
  waiting for transfers between devices  149 us (57%)
  blocking collectives  65.2 us (25%)
  local copies, waits for them, and re-layouts  17.8 us (7%)
  between operations  13.8 us (5%)
  matrix products  9.89 us (4%)
  other arithmetic  5.04 us (2%)
    all_gather x1, waiting for transfers between devices, on_device(): gathered_rows = lax.all_gather(down_local, 'fs', axis=0, tiled=True)  79.9 us
    all_to_all x1, blocking collectives, on_device(): lax.all_to_all(gathered_rows, 'tp', split_axis=0, concat_axis=1, tiled=True)  65.2 us
    all_gather x1, waiting for transfers between devices, on_device(): up_weights = lax.all_gather(up_local, 'fs', axis=0, tiled=True)  46.1 us
    reduce_scatter x1, waiting for transfers between devices, on_device(): lax.psum_scatter(jnp.dot(hidden, down_weights, preferred_element_type=jnp...  23.3 us
    unnamed x8, local copies, waits for them, and re-layouts  11.6 us
    dot_general x1, matrix products, on_device(): jnp.dot(hidden, down_weights, preferred_element_type=jnp.float32)  9.89 us
    all_to_all x1, local copies, waits for them, and re-layouts, on_device(): lax.all_to_all(gathered_rows, 'tp', split_axis=0, concat_axis=1, tiled=True)  6.21 us
  transfers between devices with their start and end apart: 4, of which 3 were waited for; matrix products, arithmetic and copies ran while one was open for 6% of the time, Pallas kernels for 0%

commit v1 on v0

v1 whole, which is shorter than its diff:
```python
import functools

import jax
import jax.numpy as jnp
from jax import lax
from jax.experimental import pallas as pl
from jax.experimental.pallas import tpu as pltpu
from jax.sharding import PartitionSpec as P

MESH = pl.DeviceIdType.MESH


def pieces(size, unit, most):
    count = most
    while count > 1 and size % (count * unit):
        count -= 1
    return count


def counts(G, F, T, r, rd, cd):
    C = pieces(r // G, 16, 2)
    J = pieces(cd, 128, 2)
    if F > 8:
        C, J = 1, 1
    return C, J, F // T


def kernel(G, F, T, C, J, m, tok_in, up_in, down_in, up_out, down_out, mlp_out,
           nrm, upw, dnw, hidden, pout, part, acc,
           send, rup, yup, rdn, ydn, rtok, rpart, loc):
    g, f, k = lax.axis_index("grp"), lax.axis_index("fs"), lax.axis_index("tp")
    r, cu = up_in.shape
    rd, cd = down_in.shape
    R, D = tok_in.shape
    h, hd, w = r // G, rd // G, cd // J
    hc = h // C
    home = f // m
    mine = k == home
    slot = f % m

    def column_owner(dev, p):
        if T % 2:
            return (dev + p) % T
        return ((dev // 2 + p // 2) % (T // 2)) * 2 + (dev + p) % 2

    def position_of(owner, dev):
        if T % 2:
            return (owner + T - dev) % T
        return ((owner // 2 + T // 2 - dev // 2) % (T // 2)) * 2 + (owner + dev) % 2

    local = []

    def keep(cond, src, dst):
        copy = pltpu.make_async_copy(src, dst, loc.at[len(local)])
        local.append(cond)
        if cond is None:
            copy.start()
        else:
            pl.when(cond)(copy.start)
        return copy

    own_up = keep(None, up_in, upw.at[pl.ds(pl.multiple_of(f * r, r), r)])
    own_tok = keep(None, tok_in, nrm.at[pl.ds(pl.multiple_of(k * R, R), R)])
    own_down = keep(mine, down_in, dnw.at[pl.ds(pl.multiple_of(slot * rd, rd), rd), pl.ds(pl.multiple_of(k * cd, cd), cd)])

    barrier = pltpu.get_barrier_semaphore()

    def greet(**where):
        pl.semaphore_signal(barrier, inc=1, device_id=where, device_id_type=MESH)

    for e in range(1, G):
        greet(grp=(g + e) % G)
    for d in range(1, T):
        greet(tp=(k + d) % T)

    @pl.when(f > 0)
    def _():
        greet(fs=f - 1)

    @pl.when(f < F - 1)
    def _():
        greet(fs=f + 1)

    pl.semaphore_wait(barrier, G - 1 + T - 1 + (f > 0).astype(jnp.int32) + (f < F - 1).astype(jnp.int32))

    sent = []

    def put(cond, src, dst, sem, where):
        copy = pltpu.make_async_remote_copy(
            src_ref=src, dst_ref=dst, send_sem=send.at[len(sent)], recv_sem=sem,
            device_id=where, device_id_type=MESH)
        sent.append((cond, copy))
        if cond is None:
            copy.start()
        else:
            pl.when(cond)(copy.start)

    def arrived(ref, sem, where):
        pltpu.make_async_remote_copy(
            src_ref=ref, dst_ref=ref, send_sem=send.at[0], recv_sem=sem,
            device_id=where, device_id_type=MESH).wait_recv()

    def up_piece(s, part_of, c):
        return upw.at[pl.ds(pl.multiple_of(s * r + part_of * h + c * hc, hc), hc)]

    def down_piece(si, p, j, part_of):
        t = column_owner(k, p)
        return dnw.at[pl.ds(pl.multiple_of(si * rd + part_of * hd, hd), hd),
                      pl.ds(pl.multiple_of(t * cd + j * w, w), w)]

    for c in range(C):
        src = up_in.at[pl.ds(pl.multiple_of(g * h + c * hc, hc), hc)]
        put(f < F - 1, src, up_piece(f, g, c), rup.at[0, 0, c], {"fs": f + 1})
        put(f > 0, src, up_piece(f, g, c), rup.at[1, 0, c], {"fs": f - 1})

    place = position_of(k, home)
    for j in range(J):
        put(jnp.logical_not(mine),
            down_in.at[pl.ds(pl.multiple_of(g * hd, hd), hd), pl.ds(j * w, w)],
            dnw.at[pl.ds(pl.multiple_of(slot * rd + g * hd, hd), hd), pl.ds(pl.multiple_of(k * cd + j * w, w), w)],
            rdn.at[slot, place, j], {"tp": home})
    for d in range(1, T):
        put(None, tok_in, nrm.at[pl.ds(pl.multiple_of(k * R, R), R)], rtok.at[d - 1], {"tp": (k + d) % T})

    own_up.wait()
    own_tok.wait()
    pl.when(mine)(own_down.wait)

    for d in range(1, F):
        for c in range(C):
            for way in range(2):
                s = f - d if way == 0 else f + d
                here = f >= d if way == 0 else f < F - d

                @pl.when(here)
                def _(s=s, way=way):
                    arrived(up_piece(s, g, c), rup.at[way, d - 1, c], {"fs": s})

                if d < F - 1:
                    more = jnp.logical_and(here, f < F - 1 if way == 0 else f > 0)
                    put(more, up_piece(s, g, c), up_piece(s, g, c), rup.at[way, d, c],
                        {"fs": f + 1 if way == 0 else f - 1})
                for e in range(1, G):
                    put(here, up_piece(s, g, c), up_piece(s, g, c), yup.at[e - 1, way, d - 1, c],
                        {"grp": (g + e) % G})

    def down_step(p, j):
        for si in range(m):
            s = k * m + si
            block = down_piece(si, p, j, g)
            away = None if p else f != s
            sem = rdn.at[si, p, j]
            if p:
                arrived(block, sem, {"fs": f})
            else:
                @pl.when(away)
                def _():
                    arrived(block, sem, {"fs": f})
            put(jnp.logical_and(f >= s, f < F - 1), block, block, sem, {"fs": f + 1})
            put(jnp.logical_and(f <= s, f > 0), block, block, sem, {"fs": f - 1})
            for e in range(1, G):
                put(away, block, block, ydn.at[e - 1, si, p, j], {"grp": (g + e) % G})

    stored = []

    def hidden_units():
        for d in range(1, F):
            for c in range(C):
                for way in range(2):
                    s = f - d if way == 0 else f + d
                    here = f >= d if way == 0 else f < F - d

                    @pl.when(here)
                    def _(s=s, way=way):
                        for e in range(1, G):
                            arrived(up_piece(s, (g + G - e) % G, c), yup.at[e - 1, way, d - 1, c], {"fs": f})

        stored.append(keep(None, upw, up_out))
        for d in range(1, T):
            arrived(nrm.at[pl.ds(pl.multiple_of((k + T - d) % T * R, R), R)], rtok.at[d - 1], {"fs": f})
        tile = min(cu, 256)

        @pl.loop(0, cu // tile)
        def _(i):
            cols = pl.ds(pl.multiple_of(i * tile, tile), tile)
            rect = jnp.maximum(jnp.dot(nrm[...], upw[:, cols], preferred_element_type=jnp.float32), 0.0)
            hidden[:, cols] = (rect * rect).astype(hidden.dtype)

    def output_step(p, j):
        for si in range(m):
            s = k * m + si

            def peers(si=si):
                for e in range(1, G):
                    arrived(down_piece(si, p, j, (g + G - e) % G), ydn.at[e - 1, si, p, j], {"fs": f})
            if p:
                peers()
            else:
                pl.when(f != s)(peers)
        cols = pl.ds(pl.multiple_of(column_owner(k, p) * cd + j * w, w), w)
        stored.append(keep(None, dnw.at[:, cols], down_out.at[:, cols]))
        pout[:, cols] = jnp.dot(hidden[...], dnw[:, cols], preferred_element_type=jnp.float32).astype(pout.dtype)
        for d in range(1, T):
            to = (k + d) % T
            put(None, pout.at[pl.ds(pl.multiple_of(to * R, R), R), cols], part.at[d - 1, :, cols],
                rpart.at[d - 1, p, j], {"tp": to})

    steps = [(p, j) for p in range(T) for j in range(J)]
    lag = min(2, len(steps))
    for n in range(len(steps) + lag):
        if n < len(steps):
            down_step(*steps[n])
        if n == lag - 1:
            hidden_units()
        if n >= lag:
            output_step(*steps[n - lag])

    for p, j in steps:
        for d in range(1, T):
            cols = pl.ds(pl.multiple_of(column_owner((k + T - d) % T, p) * cd + j * w, w), w)
            arrived(part.at[d - 1, :, cols], rpart.at[d - 1, p, j], {"fs": f})
    total = pout[pl.ds(pl.multiple_of(k * R, R), R), :].astype(jnp.float32)
    for d in range(1, T):
        total += part[d - 1].astype(jnp.float32)
    acc[...] = total.astype(acc.dtype)
    stored.append(keep(None, acc, mlp_out))
    for copy in stored:
        copy.wait()
    for cond, copy in sent:
        if cond is None:
            copy.wait_send()
        else:
            pl.when(cond)(copy.wait_send)


def solution(mesh):
    G, F, T = (mesh.shape[a] for a in ("grp", "fs", "tp"))

    def on_device(tokens, up_master, down_master, norm_gain):
        up_local = (norm_gain[:, None] * up_master).astype(jnp.bfloat16)
        down_local = down_master.astype(jnp.bfloat16)
        wide = tokens.astype(jnp.float32)
        scale = lax.rsqrt(jnp.mean(wide * wide, axis=-1, keepdims=True) + 1e-06)
        normed = (wide * scale).astype(jnp.bfloat16)
        (r, cu), (rd, cd), (R, D) = up_local.shape, down_local.shape, normed.shape
        C, J, m = counts(G, F, T, r, rd, cd)
        sends = (2 * C + J + T - 1 + 2 * (F - 1) * C * G + m * T * J * (G + 1) + T * J * (T - 1))
        bf16 = jnp.bfloat16
        dma = pltpu.SemaphoreType.DMA
        any_spec = pl.BlockSpec(memory_space=pl.ANY)
        return pl.pallas_call(
            functools.partial(kernel, G, F, T, C, J, m),
            out_shape=(
                jax.ShapeDtypeStruct((F * r, cu), bf16),
                jax.ShapeDtypeStruct((m * rd, T * cd), bf16),
                jax.ShapeDtypeStruct((R, D), bf16),
            ),
            in_specs=[any_spec] * 3,
            out_specs=(any_spec,) * 3,
            scratch_shapes=[
                pltpu.VMEM((T * R, D), bf16),
                pltpu.VMEM((F * r, cu), bf16),
                pltpu.VMEM((m * rd, T * cd), bf16),
                pltpu.VMEM((T * R, cu), bf16),
                pltpu.VMEM((T * R, D), bf16),
                pltpu.VMEM((T - 1, R, D), bf16),
                pltpu.VMEM((R, D), bf16),
                dma((sends,)),
                dma((2, F - 1, C)),
                dma((max(G - 1, 1), 2, F - 1, C)),
                dma((m, T, J)),
                dma((max(G - 1, 1), m, T, J)),
                dma((T - 1,)),
                dma((T - 1, T, J)),
                dma((5 + T * J,)),
            ],
            compiler_params=pltpu.CompilerParams(
                collective_id=0, has_side_effects=True, vmem_limit_bytes=44 * 2**20
            ),
        )(normed, up_local, down_local)

    in_specs = (P(("grp", "fs", "tp"), None), P("fs", "tp"), P("fs", "tp"), P("fs"))
    out_specs = (P("grp", "tp"), P(("grp", "tp"), None), P(("grp", "fs", "tp"), None))
    return jax.shard_map(
        on_device, mesh=mesh, in_specs=in_specs, out_specs=out_specs, check_vma=False
    )
```

time: 263 us -> 118 us (0.45)
  waiting for transfers between devices: 149 us -> 0 us
  Pallas kernels: 0 us -> 106 us
  blocking collectives: 65.2 us -> 0 us
  between operations: 13.8 us -> 0.68 us
  local copies, waits for them, and re-layouts: 17.8 us -> 6.5 us
  matrix products: 9.89 us -> 0 us
    all_gather x3 -> x0, waiting for transfers between devices: 126 us -> none  [the longest x1 79.9 us: on_device(): gathered_rows = lax.all_gather(down_local, 'fs', axis=0, tiled=True)]
    pallas_call x0 -> x1, Pallas kernels: none -> 106 us  [on_device(): pl.pallas_call(functools.partial(kernel, G, F, T, C, J, m), out_shape=(ja...]
    all_to_all x1 -> x0, blocking collectives: 65.2 us -> none  [on_device(): lax.all_to_all(gathered_rows, 'tp', split_axis=0, concat_axis=1, tiled=True)]
    reduce_scatter x1 -> x0, waiting for transfers between devices: 23.3 us -> none  [on_device(): lax.psum_scatter(jnp.dot(hidden, down_weights, preferred_element_type=jnp...]
    dot_general x1 -> x0, matrix products: 9.89 us -> none  [on_device(): jnp.dot(hidden, down_weights, preferred_element_type=jnp.float32)]
    all_to_all x1 -> x0, local copies, waits for them, and re-layouts: 6.21 us -> none  [on_device(): lax.all_to_all(gathered_rows, 'tp', split_axis=0, concat_axis=1, tiled=True)]
    unnamed x8 -> x7, local copies, waits for them, and re-layouts: 11.6 us -> 6.5 us
  transfers between devices with their start and end apart: 4 -> 0, of which waited for: 3 -> 0; matrix products, arithmetic and copies ran while one was open for 6% -> 0% of each run, Pallas kernels for 0% -> 0%
where the time goes in v1:
time: 118 us
  Pallas kernels  106 us (90%)
  local copies, waits for them, and re-layouts  6.5 us (6%)
  other arithmetic  4.49 us (4%)
    pallas_call x1, Pallas kernels, on_device(): pl.pallas_call(functools.partial(kernel, G, F, T, C, J, m), out_shape=(ja...  106 us
    unnamed x7, local copies, waits for them, and re-layouts  6.5 us

profile of v1, /device:TPU:1, one launch (start us, length us, event | category | flops | bytes accessed | tf_op | source)
XLA Modules:
  0.0 117.9 jit_solution(2850889043153851238)
XLA Ops:
  0.6 1.2 %fusion = f32[128]{0:T(128)S(1)} fusion(bf16[128,2048]{1,0:T(8,128)(2,1)} %param.4), kind=kLoop, calls=%fused_computation.3 | loop fusion | flops 786304 | bytes 524800 | tf_op jit(solution)/shard_map/reduce_sum | solution.py:243
  1.9 0.0 copy-start.1
  1.9 1.3 %fusion.1.tok_in = bf16[128,2048]{1,0:T(8,128)(2,1)S(1)} fusion(bf16[128,2048]{1,0:T(8,128)(2,1)} %param.4, f32[128]{0:T(128)S(1)} %add_rsqrt_fusion), kind=kLoop, calls=%fused_computation.4 | loop fusion | flops 786432 | bytes 1049088 | tf_op jit(solution)/shard_map/convert_element_type | solution.py:244
  3.2 1.8 %multiply_convert_fusion.up_in = bf16[512,1024]{1,0:T(8,128)(2,1)S(1)} fusion(f32[512,1024]{1,0:T(8,128)} %param.5, f32[512]{0:T(512)} %param.7), kind=kLoop, calls=%fused_computation | loop fusion | flops 1048576 | bytes 3147776 | tf_op jit(solution)/shard_map/convert_element_type | solution.py:240
  5.0 0.0 copy-done.1
  5.0 0.1 convert_element_type.15.down_in
  5.2 106.2 %shard_map.67 = (bf16[2048,1024]{1,0:T(8,128)(2,1)S(1)}, bf16[1024,2048]{1,0:T(8,128)(2,1)}, bf16[128,2048]{1,0:T(8,128)(2,1)S(1)}) custom-call(bf16[128,2048]{1,0:T(8,128)(2,1)S(1)} %fusion.1.tok_in, bf16[512,1024]{1,0:T(8,128)(2,1)S(1)} %multiply_convert_fusion.up_in, bf16[1024,512]{1,0:T(8,128)(2,1)S(1)} %convert_element_type.15.down_in), custom_call_target="tpu_custom_call" | custom-call | tf_op jit(solution)/shard_map/pallas_call | solution.py:251
  111.4 0.0 copy-start
  111.4 2.1 %copy.10 = bf16[2048,1024]{1,0:T(8,128)(2,1)} copy(bf16[2048,1024]{1,0:T(8,128)(2,1)S(1)} %get-tuple-element.6) | data formatting | bytes 8388608
  113.5 1.6 %copy-done = bf16[1024,2048]{1,0:T(8,128)(2,1)S(1)} copy-done((bf16[1024,2048]{1,0:T(8,128)(2,1)S(1)}, bf16[1024,2048]{1,0:T(8,128)(2,1)}, u32[]{:S(2)}) %copy-start) | copy-done | bytes 4194328
  115.1 2.0 %copy.11 = bf16[1024,2048]{1,0:T(8,128)(2,1)} copy(bf16[1024,2048]{1,0:T(8,128)(2,1)S(1)} %copy-done) | data formatting | bytes 8388608
  117.1 0.8 copy.12
  (1 shorter events, 0.0 us)
Async XLA Ops:
  1.9 3.1 %copy-start.1 = (f32[1024,512]{1,0:T(8,128)S(1)}, f32[1024,512]{1,0:T(8,128)}, u32[]{:S(2)}) copy-start(f32[1024,512]{1,0:T(8,128)} %param.6) | copy-start | bytes 6291460
  111.4 3.7 %copy-start = (bf16[1024,2048]{1,0:T(8,128)(2,1)S(1)}, bf16[1024,2048]{1,0:T(8,128)(2,1)}, u32[]{:S(2)}) copy-start(bf16[1024,2048]{1,0:T(8,128)(2,1)} %get-tuple-element.7) | copy-start | bytes 12582916

commit v2 on v1

--- a/solution.py
+++ b/solution.py
@@ -8,6 +8,9 @@
 from jax.sharding import PartitionSpec as P
 
 MESH = pl.DeviceIdType.MESH
+DETOUR = False
+FINAL = True
+VMEM_MIB = 36
 
 
 def pieces(size, unit, most):
@@ -25,9 +28,10 @@
     return C, J, F // T
 
 
-def kernel(G, F, T, C, J, m, tok_in, up_in, down_in, up_out, down_out, mlp_out,
+def kernel(G, F, T, C, J, m, detour, gain, tok_in, up_in, down_in, up_out, down_out, mlp_out,
+           wide_up, wide_down, raw_tok, stage, alt,
            nrm, upw, dnw, hidden, pout, part, acc,
-           send, rup, yup, rdn, ydn, rtok, rpart, loc):
+           send, rup, yup, rdn, ydn, rtok, rpart, ralt, yalt, loc):
     g, f, k = lax.axis_index("grp"), lax.axis_index("fs"), lax.axis_index("tp")
     r, cu = up_in.shape
     rd, cd = down_in.shape
@@ -59,9 +63,9 @@
             pl.when(cond)(copy.start)
         return copy
 
-    own_up = keep(None, up_in, upw.at[pl.ds(pl.multiple_of(f * r, r), r)])
-    own_tok = keep(None, tok_in, nrm.at[pl.ds(pl.multiple_of(k * R, R), R)])
-    own_down = keep(mine, down_in, dnw.at[pl.ds(pl.multiple_of(slot * rd, rd), rd), pl.ds(pl.multiple_of(k * cd, cd), cd)])
+    load_up = keep(None, up_in, wide_up)
+    load_down = keep(None, down_in, wide_down)
+    load_tok = keep(None, tok_in, raw_tok)
 
     barrier = pltpu.get_barrier_semaphore()
 
@@ -81,6 +85,31 @@
     def _():
         greet(fs=f + 1)
 
+    def scale_up(half):
+        rows = min(h, 128)
+        for a in range(0, h, rows):
+            at = pl.multiple_of(half * h + a, rows)
+            column = jnp.broadcast_to(gain[:, pl.ds(at, rows)], (128, rows)).T if rows == 128 else None
+            for b in range(0, cu, 128):
+                block = wide_up[pl.ds(at, rows), pl.ds(b, 128)]
+                factor = column if column is not None else gain_column(at, rows)
+                upw[pl.ds(pl.multiple_of(f * r + at, rows), rows), pl.ds(b, 128)] = (factor * block).astype(upw.dtype)
+
+    def gain_column(at, rows):
+        lanes = lax.broadcasted_iota(jnp.int32, (rows, r), 1)
+        row = lax.broadcasted_iota(jnp.int32, (rows, r), 0)
+        picked = jnp.where(lanes == row + at, gain[...], 0.0)
+        return jnp.sum(picked, axis=1, keepdims=True)
+
+    def round_down(half):
+        rows = pl.ds(pl.multiple_of(half * hd, hd), hd)
+        for j in range(J):
+            stage[j, rows, :] = wide_down[rows, pl.ds(j * w, w)].astype(stage.dtype)
+
+    load_up.wait()
+    scale_up(g)
+    load_down.wait()
+    round_down(g)
     pl.semaphore_wait(barrier, G - 1 + T - 1 + (f > 0).astype(jnp.int32) + (f < F - 1).astype(jnp.int32))
 
     sent = []
@@ -105,26 +134,80 @@
 
     def down_piece(si, p, j, part_of):
         t = column_owner(k, p)
-        return dnw.at[pl.ds(pl.multiple_of(si * rd + part_of * hd, hd), hd),
-                      pl.ds(pl.multiple_of(t * cd + j * w, w), w)]
-
+        return dnw.at[t * J + j, pl.ds(pl.multiple_of(si * rd + part_of * hd, hd), hd)]
+
+    if detour:
+        via = ((k // 2 + 1) % (T // 2)) * 2 + (k + 1) % 2
+        upward = 2 * via < T
+        passing = jnp.logical_or(jnp.logical_and(upward, f > via), jnp.logical_and(jnp.logical_not(upward), f < via))
     for c in range(C):
-        src = up_in.at[pl.ds(pl.multiple_of(g * h + c * hc, hc), hc)]
+        src = up_piece(f, g, c)
         put(f < F - 1, src, up_piece(f, g, c), rup.at[0, 0, c], {"fs": f + 1})
         put(f > 0, src, up_piece(f, g, c), rup.at[1, 0, c], {"fs": f - 1})
+        if detour and c == 0:
+            for j in range(J):
+                src = stage.at[j, pl.ds(pl.multiple_of(g * hd, hd), hd)]
+                dst = alt.at[j, pl.ds(pl.multiple_of(g * hd, hd), hd)]
+                put(jnp.logical_and(upward, jnp.logical_and(f == via, f < F - 1)), src, dst, ralt.at[j], {"fs": f + 1})
+                put(jnp.logical_and(jnp.logical_not(upward), jnp.logical_and(f == via, f > 0)), src, dst, ralt.at[j], {"fs": f - 1})
 
     place = position_of(k, home)
     for j in range(J):
-        put(jnp.logical_not(mine),
-            down_in.at[pl.ds(pl.multiple_of(g * hd, hd), hd), pl.ds(j * w, w)],
-            dnw.at[pl.ds(pl.multiple_of(slot * rd + g * hd, hd), hd), pl.ds(pl.multiple_of(k * cd + j * w, w), w)],
+        put(jnp.logical_not(mine), stage.at[j, pl.ds(pl.multiple_of(g * hd, hd), hd)],
+            dnw.at[k * J + j, pl.ds(pl.multiple_of(slot * rd + g * hd, hd), hd)],
             rdn.at[slot, place, j], {"tp": home})
-    for d in range(1, T):
-        put(None, tok_in, nrm.at[pl.ds(pl.multiple_of(k * R, R), R)], rtok.at[d - 1], {"tp": (k + d) % T})
-
-    own_up.wait()
-    own_tok.wait()
-    pl.when(mine)(own_down.wait)
+
+    for e in range(1, G):
+        scale_up((g + e) % G)
+        round_down((g + e) % G)
+    load_tok.wait()
+    wide = raw_tok[...].astype(jnp.float32)
+    mean = jnp.mean(wide * wide, axis=-1, keepdims=True)
+    nrm[pl.ds(pl.multiple_of(k * R, R), R), :] = (wide * lax.rsqrt(mean + 1e-06)).astype(nrm.dtype)
+    held = [keep(mine, stage.at[j], dnw.at[k * J + j, pl.ds(pl.multiple_of(slot * rd, rd), rd)]) for j in range(J)]
+    for copy in held:
+        pl.when(mine)(copy.wait)
+    def tokens_of(owner):
+        return nrm.at[pl.ds(pl.multiple_of(owner * R, R), R)]
+
+    own = tokens_of(k)
+    if T % 2:
+        for p in range(1, T):
+            put(None, own, own, rtok.at[T - p], {"tp": column_owner(k, p)})
+    else:
+        for p in range(2, T, 2):
+            put(None, own, own, rtok.at[T - p], {"tp": column_owner(k, p)})
+        put(None, own, own, rtok.at[1], {"tp": column_owner(k, 1)})
+
+    def pass_tokens():
+        if T % 2 == 0:
+            for p in range(2, T, 2):
+                block = tokens_of(column_owner(k, p))
+                arrived(block, rtok.at[p], {"fs": f})
+                put(None, block, block, rtok.at[p + 1], {"tp": column_owner(k, 1)})
+
+    def alt_step(j):
+        block = alt.at[j, pl.ds(pl.multiple_of(g * hd, hd), hd)]
+
+        @pl.when(passing)
+        def _():
+            arrived(block, ralt.at[j], {"fs": f})
+
+        put(jnp.logical_and(passing, jnp.logical_and(upward, f < F - 1)), block, block, ralt.at[j], {"fs": f + 1})
+        put(jnp.logical_and(passing, jnp.logical_and(jnp.logical_not(upward), f > 0)), block, block, ralt.at[j], {"fs": f - 1})
+        for e in range(1, G):
+            put(passing, block, block, yalt.at[e - 1, j], {"grp": (g + e) % G})
+        put(passing, block, dnw.at[k * J + j, pl.ds(pl.multiple_of(g * hd, hd), hd)], rdn.at[0, T - 1, j], {"tp": via})
+
+    def alt_cross(j):
+        for e in range(1, G):
+            rows = pl.ds(pl.multiple_of((g + G - e) % G * hd, hd), hd)
+
+            @pl.when(passing)
+            def _():
+                arrived(alt.at[j, rows], yalt.at[e - 1, j], {"fs": f})
+
+            put(passing, alt.at[j, rows], dnw.at[k * J + j, rows], ydn.at[e - 1, 0, T - 1, j], {"tp": via})
 
     for d in range(1, F):
         for c in range(C):
@@ -143,6 +226,15 @@
                 for e in range(1, G):
                     put(here, up_piece(s, g, c), up_piece(s, g, c), yup.at[e - 1, way, d - 1, c],
                         {"grp": (g + e) % G})
+
+        if d == min(2, F - 1):
+            pass_tokens()
+        if detour:
+            for j in range(J):
+                if d == 1:
+                    alt_step(j)
+                if d == min(2, F - 1):
+                    alt_cross(j)
 
     def down_step(p, j):
         for si in range(m):
@@ -156,8 +248,16 @@
                 @pl.when(away)
                 def _():
                     arrived(block, sem, {"fs": f})
-            put(jnp.logical_and(f >= s, f < F - 1), block, block, sem, {"fs": f + 1})
-            put(jnp.logical_and(f <= s, f > 0), block, block, sem, {"fs": f - 1})
+            right = jnp.logical_and(f >= s, f < F - 1)
+            left = jnp.logical_and(f <= s, f > 0)
+            if detour and p == T - 1:
+                low = 2 * k < T
+                high = jnp.logical_not(low)
+                right = jnp.logical_and(right, high)
+                left = jnp.logical_and(left, low)
+                away = jnp.logical_and(jnp.logical_or(high, f <= s), jnp.logical_or(low, f >= s))
+            put(right, block, block, sem, {"fs": f + 1})
+            put(left, block, block, sem, {"fs": f - 1})
             for e in range(1, G):
                 put(away, block, block, ydn.at[e - 1, si, p, j], {"grp": (g + e) % G})
 
@@ -176,8 +276,9 @@
                             arrived(up_piece(s, (g + G - e) % G, c), yup.at[e - 1, way, d - 1, c], {"fs": f})
 
         stored.append(keep(None, upw, up_out))
-        for d in range(1, T):
-            arrived(nrm.at[pl.ds(pl.multiple_of((k + T - d) % T * R, R), R)], rtok.at[d - 1], {"fs": f})
+        for p in range(1, T):
+            if T % 2 or p % 2:
+                arrived(tokens_of(column_owner(k, p)), rtok.at[p], {"fs": f})
         tile = min(cu, 256)
 
         @pl.loop(0, cu // tile)
@@ -197,32 +298,38 @@
                 peers()
             else:
                 pl.when(f != s)(peers)
-        cols = pl.ds(pl.multiple_of(column_owner(k, p) * cd + j * w, w), w)
-        stored.append(keep(None, dnw.at[:, cols], down_out.at[:, cols]))
-        pout[:, cols] = jnp.dot(hidden[...], dnw[:, cols], preferred_element_type=jnp.float32).astype(pout.dtype)
+        n = column_owner(k, p) * J + j
+        stored.append(keep(None, dnw.at[n], down_out.at[:, pl.ds(pl.multiple_of(n * w, w), w)]))
+        pout[n] = jnp.dot(hidden[...], dnw[n], preferred_element_type=jnp.float32).astype(pout.dtype)
         for d in range(1, T):
             to = (k + d) % T
-            put(None, pout.at[pl.ds(pl.multiple_of(to * R, R), R), cols], part.at[d - 1, :, cols],
+            put(None, pout.at[n, pl.ds(pl.multiple_of(to * R, R), R)], part.at[d - 1, n],
                 rpart.at[d - 1, p, j], {"tp": to})
 
     steps = [(p, j) for p in range(T) for j in range(J)]
-    lag = min(2, len(steps))
-    for n in range(len(steps) + lag):
-        if n < len(steps):
-            down_step(*steps[n])
-        if n == lag - 1:
+    first = min(4, len(steps)) - 1
+    done = 0
+    for n in range(len(steps)):
+        down_step(*steps[n])
+        if n == first:
             hidden_units()
-        if n >= lag:
-            output_step(*steps[n - lag])
+        if n >= first:
+            while done < n - 1:
+                output_step(*steps[done])
+                done += 1
+    for step in steps[done:]:
+        output_step(*step)
 
     for p, j in steps:
         for d in range(1, T):
-            cols = pl.ds(pl.multiple_of(column_owner((k + T - d) % T, p) * cd + j * w, w), w)
-            arrived(part.at[d - 1, :, cols], rpart.at[d - 1, p, j], {"fs": f})
-    total = pout[pl.ds(pl.multiple_of(k * R, R), R), :].astype(jnp.float32)
-    for d in range(1, T):
-        total += part[d - 1].astype(jnp.float32)
-    acc[...] = total.astype(acc.dtype)
+            n = column_owner((k + T - d) % T, p) * J + j
+            arrived(part.at[d - 1, n], rpart.at[d - 1, p, j], {"fs": f})
+    own_rows = pl.ds(pl.multiple_of(k * R, R), R)
+    for n in range(T * J):
+        total = pout[n, own_rows, :].astype(jnp.float32)
+        for d in range(1, T):
+            total += part[d - 1, n].astype(jnp.float32)
+        acc[:, n * w:(n + 1) * w] = total.astype(acc.dtype)
     stored.append(keep(None, acc, mlp_out))
     for copy in stored:
         copy.wait()
@@ -233,51 +340,73 @@
             pl.when(cond)(copy.wait_send)
 
 
+def place(a, b, c, x, y, z, sems):
+    copies = [pltpu.make_async_copy(i, o, sems.at[n]) for n, (i, o) in enumerate(((a, x), (b, y), (c, z)))]
+    for copy in copies:
+        copy.start()
+    for copy in copies:
+        copy.wait()
+
+
 def solution(mesh):
     G, F, T = (mesh.shape[a] for a in ("grp", "fs", "tp"))
 
     def on_device(tokens, up_master, down_master, norm_gain):
-        up_local = (norm_gain[:, None] * up_master).astype(jnp.bfloat16)
-        down_local = down_master.astype(jnp.bfloat16)
-        wide = tokens.astype(jnp.float32)
-        scale = lax.rsqrt(jnp.mean(wide * wide, axis=-1, keepdims=True) + 1e-06)
-        normed = (wide * scale).astype(jnp.bfloat16)
-        (r, cu), (rd, cd), (R, D) = up_local.shape, down_local.shape, normed.shape
+        (r, cu), (rd, cd), (R, D) = up_master.shape, down_master.shape, tokens.shape
         C, J, m = counts(G, F, T, r, rd, cd)
-        sends = (2 * C + J + T - 1 + 2 * (F - 1) * C * G + m * T * J * (G + 1) + T * J * (T - 1))
+        w = cd // J
+        detour = DETOUR and m == 1 and T % 2 == 0 and T > 2
+        sends = 2 * J + J * (2 * G + 2) + (2 * C + J + T - 1 + 2 * (F - 1) * C * G + m * T * J * (G + 1) + T * J * (T - 1))
         bf16 = jnp.bfloat16
         dma = pltpu.SemaphoreType.DMA
         any_spec = pl.BlockSpec(memory_space=pl.ANY)
-        return pl.pallas_call(
-            functools.partial(kernel, G, F, T, C, J, m),
+        held = pl.pallas_call(
+            functools.partial(kernel, G, F, T, C, J, m, detour),
             out_shape=(
                 jax.ShapeDtypeStruct((F * r, cu), bf16),
                 jax.ShapeDtypeStruct((m * rd, T * cd), bf16),
                 jax.ShapeDtypeStruct((R, D), bf16),
             ),
-            in_specs=[any_spec] * 3,
+            in_specs=[pl.BlockSpec(memory_space=pltpu.VMEM)] + [pl.BlockSpec(memory_space=pltpu.HBM)] * 3,
             out_specs=(any_spec,) * 3,
             scratch_shapes=[
+                pltpu.VMEM((r, cu), jnp.float32),
+                pltpu.VMEM((rd, cd), jnp.float32),
+                pltpu.VMEM((R, D), bf16),
+                pltpu.VMEM((J, rd, w), bf16),
+                pltpu.VMEM((J, rd, w), bf16),
                 pltpu.VMEM((T * R, D), bf16),
                 pltpu.VMEM((F * r, cu), bf16),
-                pltpu.VMEM((m * rd, T * cd), bf16),
+                pltpu.VMEM((T * J, m * rd, w), bf16),
                 pltpu.VMEM((T * R, cu), bf16),
-                pltpu.VMEM((T * R, D), bf16),
-                pltpu.VMEM((T - 1, R, D), bf16),
+                pltpu.VMEM((T * J, T * R, w), bf16),
+                pltpu.VMEM((T - 1, T * J, R, w), bf16),
                 pltpu.VMEM((R, D), bf16),
                 dma((sends,)),
                 dma((2, F - 1, C)),
                 dma((max(G - 1, 1), 2, F - 1, C)),
                 dma((m, T, J)),
                 dma((max(G - 1, 1), m, T, J)),
-                dma((T - 1,)),
+                dma((T,)),
                 dma((T - 1, T, J)),
-                dma((5 + T * J,)),
+                dma((J,)),
+                dma((max(G - 1, 1), J)),
+                dma((5 + J + T * J,)),
             ],
             compiler_params=pltpu.CompilerParams(
-                collective_id=0, has_side_effects=True, vmem_limit_bytes=44 * 2**20
+                collective_id=0, has_side_effects=True, vmem_limit_bytes=VMEM_MIB * 2**20
             ),
-        )(normed, up_local, down_local)
+        )(norm_gain.reshape(1, r), tokens, up_master, down_master)
+        if not FINAL:
+            return held
+        return pl.pallas_call(
+            place,
+            out_shape=tuple(jax.ShapeDtypeStruct(a.shape, a.dtype) for a in held),
+            in_specs=[any_spec] * 3,
+            out_specs=(any_spec,) * 3,
+            scratch_shapes=[dma((3,))],
+            compiler_params=pltpu.CompilerParams(vmem_limit_bytes=2**20),
+        )(*held)
 
     in_specs = (P(("grp", "fs", "tp"), None), P("fs", "tp"), P("fs", "tp"), P("fs"))
     out_specs = (P("grp", "tp"), P(("grp", "tp"), None), P(("grp", "fs", "tp"), None))

time: 118 us -> 109 us (0.924)
  other arithmetic: 4.49 us -> 0 us
  Pallas kernels: 106 us -> 104 us
  local copies, waits for them, and re-layouts: 6.5 us -> 4.9 us
    convert_element_type x3 -> x0, other arithmetic: 3.25 us -> none  [the longest x1 1.77 us: on_device(): up_local = (norm_gain[:, None] * up_master).astype(jnp.bfloat16)]
    pallas_call x1 -> x2, Pallas kernels: 106 us -> 104 us  [the longest x1 100 us: on_device(): pl.pallas_call(functools.partial(kernel, G, F, T, C, J, m, detour), out_s...]
    unnamed x7 -> x8, local copies, waits for them, and re-layouts: 6.5 us -> 4.9 us
    reduce_sum x1 -> x0, other arithmetic: 1.23 us -> none  [on_device(): scale = lax.rsqrt(jnp.mean(wide * wide, axis=-1, keepdims=True) + 1e-06)]
where the time goes in v2:
time: 109 us
  Pallas kernels  104 us (95%)
  local copies, waits for them, and re-layouts  4.9 us (4%)
    pallas_call x1, Pallas kernels, on_device(): pl.pallas_call(functools.partial(kernel, G, F, T, C, J, m, detour), out_s...  100 us
    unnamed x8, local copies, waits for them, and re-layouts  4.9 us
    pallas_call x1, Pallas kernels, on_device(): pl.pallas_call(place, out_shape=tuple((jax.ShapeDtypeStruct(a.shape, a.dt...  3.46 us

profile of v2, /device:TPU:1, one launch (start us, length us, event | category | flops | bytes accessed | tf_op | source)
XLA Modules:
  0.0 109.1 jit_solution(14946917182530844134)
XLA Ops:
  0.6 0.0 copy-start
  0.6 1.6 %copy-done = f32[512,1024]{1,0:T(8,128)S(1)} copy-done((f32[512,1024]{1,0:T(8,128)S(1)}, f32[512,1024]{1,0:T(8,128)}, u32[]{:S(2)}) %copy-start) | copy-done | bytes 2097176
  2.2 0.0 copy-start.1
  2.2 1.6 %copy-done.1 = f32[1024,512]{1,0:T(8,128)S(1)} copy-done((f32[1024,512]{1,0:T(8,128)S(1)}, f32[1024,512]{1,0:T(8,128)}, u32[]{:S(2)}) %copy-start.1) | copy-done | bytes 2097176
  3.8 0.0 copy-start.2
  3.8 1.0 copy-done.2
  4.9 0.0 copy-start.3
  4.9 0.7 copy-done.3
  5.5 100.1 %shard_map.67 = (bf16[2048,1024]{1,0:T(8,128)(2,1)S(1)}, bf16[1024,2048]{1,0:T(8,128)(2,1)S(1)}, bf16[128,2048]{1,0:T(8,128)(2,1)S(1)}) custom-call(f32[1,512]{1,0:T(1,128)S(1)} %bitcast.1, bf16[128,2048]{1,0:T(8,128)(2,1)S(1)} %copy-done.2, f32[512,1024]{1,0:T(8,128)S(1)} %copy-done, f32[1024,512]{1,0:T(8,128)S(1)} %copy-done.1), custom_call_target="tpu_custom_call" | custom-call | tf_op jit(solution)/shard_map/pallas_call | solution.py:363
  105.7 3.5 %shard_map.68 = (bf16[2048,1024]{1,0:T(8,128)(2,1)}, bf16[1024,2048]{1,0:T(8,128)(2,1)}, bf16[128,2048]{1,0:T(8,128)(2,1)}) custom-call(bf16[2048,1024]{1,0:T(8,128)(2,1)S(1)} %get-tuple-element.6.a, bf16[1024,2048]{1,0:T(8,128)(2,1)S(1)} %get-tuple-element.7.b, bf16[128,2048]{1,0:T(8,128)(2,1)S(1)} %get-tuple-element.8.c), custom_call_target="tpu_custom_call" | custom-call | tf_op jit(solution)/shard_map/pallas_call | solution.py:402
Async XLA Ops:
  0.6 1.6 %copy-start = (f32[512,1024]{1,0:T(8,128)S(1)}, f32[512,1024]{1,0:T(8,128)}, u32[]{:S(2)}) copy-start(f32[512,1024]{1,0:T(8,128)} %up_in.1) | copy-start | bytes 6291460
  2.2 1.6 %copy-start.1 = (f32[1024,512]{1,0:T(8,128)S(1)}, f32[1024,512]{1,0:T(8,128)}, u32[]{:S(2)}) copy-start(f32[1024,512]{1,0:T(8,128)} %down_in.1) | copy-start | bytes 6291460
  3.8 1.0 copy-start.2
  4.9 0.7 copy-start.3
